TPU v7x, 512 devices: a whole 4x8x8 slice. The times are simulated.
512 devices in a mesh: ep: 32 (over z, x), tp: 16 (over y, core).
Axes of the slice: x: 4, y: 8, z: 8, core: 2. Of those that a mesh axis runs over, the one named last changes fastest.
Arguments:
- tokens: bfloat16 [4096, 4096], P('ep', 'tp'), may hold values from -6 to 6
- cotangent: bfloat16 [4096, 4096], P('ep', 'tp'), may hold values from -6 to 6
- routes: int32 [4096, 2], P('ep'), may hold values from 0 to 31, all different within a row; in each aligned block of 128 rows (0 to 127, 128 to 255, ...) at most 12 rows name the same one
- gate_weight: float32 [4096, 2], P('ep'), may hold values from 0.1 to 2.5
- w_gate: bfloat16 [32, 1024, 4096], P('ep', 'tp'), may hold values from -0.09375 to 0.09375
- w_up: bfloat16 [32, 1024, 4096], P('ep', 'tp'), may hold values from -0.09375 to 0.09375
- w_down: bfloat16 [32, 1024, 4096], P('ep', 'tp'), may hold values from -0.1875 to 0.1875
- shared_hidden: bfloat16 [4096, 1024], P('ep'), may hold values from -4 to 4
Outputs:
- tokens_grad: bfloat16 [4096, 4096], P('ep', 'tp')
- gate_grad: float32 [4096, 2], P('ep')
- w_gate_grad: float32 [32, 1024, 4096], P('ep', 'tp')
- w_up_grad: float32 [32, 1024, 4096], P('ep', 'tp')
- w_down_grad: float32 [32, 1024, 4096], P('ep', 'tp')
- shared_grad: float32 [1024, 4096], P('ep', 'tp')
Inputs may be any that keep to these rules, and one draw needn't show every extreme that they name: `routes`: each row names 2 different experts. Among the rows of one index of ep (aligned blocks of 128 rows) no expert is named more than 12 times, and in every draw some expert is named exactly 12 times in some block.
All inputs are finite; a program needn't handle non-finite values.
Results may differ from a plain program's by a relative error of at most 0.022.
Values may be sent and summed in bfloat16 or wider, within the bound.
A program may use at most 64 MiB of HBM per device.

v0:
```python
import jax
import jax.numpy as jnp
from jax import lax
from jax.sharding import PartitionSpec as P


def in_one_piece(arrays, axis, dim, along):
    ends, at = ([], 0)
    for a in arrays[:-1]:
        at += a.shape[along]
        ends.append(at)
    both = jnp.concatenate(arrays, axis=along)
    return tuple(jnp.split(lax.all_gather(both, axis, axis=dim, tiled=True), ends, axis=along))


def from_everyone(array, axis):
    copies = jnp.broadcast_to(array, (lax.axis_size(axis), *array.shape))
    return lax.all_to_all(copies, axis, split_axis=0, concat_axis=0, tiled=True)


def taken_together(array, axis):
    everything = from_everyone(array, axis)
    return jnp.sum(everything, axis=0)


def in_blocks(array, dim, size):
    before, after = (array.shape[:dim], array.shape[dim + 1 :])
    return jnp.moveaxis(array.reshape(*before, size, -1, *after), dim, 0)


def sent_and_summed(array, axis, dim):
    pieces = in_blocks(array, dim, lax.axis_size(axis))
    arrived = lax.all_to_all(pieces, axis, split_axis=0, concat_axis=0, tiled=True)
    return arrived.astype(jnp.float32).sum(axis=0)


def slot_positions(flat_routes, experts):
    onehot = (flat_routes[:, None] == jnp.arange(experts, dtype=jnp.int32)[None, :]).astype(
        jnp.int32
    )
    earlier = jnp.cumsum(onehot, axis=0) - onehot
    return jnp.sum(earlier * onehot, axis=1)


def shards(tokens, cotangent, routes, gate_weight, w_gate, w_up, w_down, shared_hidden):
    tok_count, top_count = routes.shape
    experts = lax.axis_size("ep")
    capacity = 3 * tok_count * top_count // (2 * experts)
    flat_routes = routes.reshape(-1)
    positions = slot_positions(flat_routes, experts)
    token_ids = jnp.arange(tok_count * top_count, dtype=jnp.int32) // top_count
    slot_table = (
        jnp.full((experts, capacity), tok_count, jnp.int32)
        .at[flat_routes, positions]
        .set(token_ids)
    )
    weight_table = (
        jnp.zeros((experts, capacity), jnp.float32)
        .at[flat_routes, positions]
        .set(gate_weight.reshape(-1))
    )

    def place_rows(source_rows):
        padded = jnp.concatenate(
            [source_rows, jnp.zeros((1, source_rows.shape[1]), source_rows.dtype)], 0
        )
        return padded[slot_table]

    part_tokens, part_cotan, recv_weight = (
        lax.all_to_all(place_rows(tokens), "ep", split_axis=0, concat_axis=0, tiled=True),
        lax.all_to_all(place_rows(cotangent), "ep", split_axis=0, concat_axis=0, tiled=True),
        lax.all_to_all(
            weight_table.astype(jnp.bfloat16), "ep", split_axis=0, concat_axis=0, tiled=True
        ).astype(weight_table.dtype),
    )
    recv_tokens, recv_cotan = in_one_piece((part_tokens, part_cotan), "tp", 2, 0)
    row_total = experts * capacity
    width = recv_tokens.shape[2]
    contract_last = (((1,), (1,)), ((), ()))
    rows_x = recv_tokens.reshape(row_total, width)
    rows_g = recv_cotan.reshape(row_total, width)
    weight_col = recv_weight.reshape(row_total, 1)
    gate_mat = w_gate[0]
    up_mat = w_up[0]
    down_mat = w_down[0]
    pre_gate = lax.dot_general(rows_x, gate_mat, contract_last, preferred_element_type=jnp.float32)
    pre_up = lax.dot_general(rows_x, up_mat, contract_last, preferred_element_type=jnp.float32)
    sigmoid_gate = jax.nn.sigmoid(pre_gate)
    silu_gate = pre_gate * sigmoid_gate
    hidden = (silu_gate * pre_up).astype(jnp.bfloat16)
    back_hidden = lax.dot_general(
        rows_g, down_mat, contract_last, preferred_element_type=jnp.float32
    )
    gate_part = jnp.sum(hidden.astype(jnp.float32) * back_hidden, axis=1)
    scaled = weight_col * back_hidden
    grad_pre_gate = (
        scaled * pre_up * sigmoid_gate * (1.0 + pre_gate * (1.0 - sigmoid_gate))
    ).astype(jnp.bfloat16)
    grad_pre_up = (scaled * silu_gate).astype(jnp.bfloat16)
    weighted_cotan = (weight_col * rows_g.astype(jnp.float32)).astype(jnp.bfloat16)
    grad_down = jnp.dot(hidden.T, weighted_cotan, preferred_element_type=jnp.float32)
    grad_gate = jnp.dot(grad_pre_gate.T, rows_x, preferred_element_type=jnp.float32)
    grad_up = jnp.dot(grad_pre_up.T, rows_x, preferred_element_type=jnp.float32)
    partial_value = jnp.dot(grad_pre_gate, gate_mat, preferred_element_type=jnp.float32)
    partial_value = partial_value + jnp.dot(grad_pre_up, up_mat, preferred_element_type=jnp.float32)
    rounded = lax.optimization_barrier(partial_value.astype(jnp.bfloat16)).astype(jnp.float32)
    row_share = lax.psum_scatter(
        rounded.reshape(experts, capacity, width).astype(jnp.bfloat16),
        "tp",
        scatter_dimension=2,
        tiled=True,
    )
    gate_total = taken_together(gate_part.reshape(experts, capacity), "tp")
    back_rows, back_gate = (
        lax.all_to_all(row_share, "ep", split_axis=0, concat_axis=0, tiled=True),
        lax.all_to_all(
            gate_total.astype(jnp.bfloat16), "ep", split_axis=0, concat_axis=0, tiled=True
        ).astype(gate_total.dtype),
    )
    picked = back_rows[flat_routes, positions].astype(jnp.float32)
    tokens_grad = jnp.sum(picked.reshape(tok_count, top_count, -1), axis=1).astype(jnp.bfloat16)
    gate_grad = back_gate[flat_routes, positions].reshape(tok_count, top_count)
    shared_grad = sent_and_summed(
        jnp.dot(shared_hidden.T, cotangent, preferred_element_type=jnp.float32).astype(
            jnp.bfloat16
        ),
        "ep",
        0,
    )
    return (tokens_grad, gate_grad, grad_gate[None], grad_up[None], grad_down[None], shared_grad)


def solution(mesh):
    placed = (
        P("ep", "tp"),
        P("ep", "tp"),
        P("ep", None),
        P("ep", None),
        P("ep", "tp", None),
        P("ep", "tp", None),
        P("ep", "tp", None),
        P("ep", None),
    )
    return jax.shard_map(
        shards,
        mesh=mesh,
        in_specs=placed,
        out_specs=(
            P("ep", "tp"),
            P("ep", None),
            P("ep", "tp", None),
            P("ep", "tp", None),
            P("ep", "tp", None),
            P("ep", "tp"),
        ),
        check_vma=False,
    )
```

profile of v0, /device:TPU:1, one launch (start us, length us, event | category | flops | bytes accessed | tf_op | source)
XLA Modules:
  0.0 257.8 jit_solution(6371332062408701905)
XLA Ops:
  9.5 12.8 %scatter_fusion.1 = s32[32,12]{0,1:T(8,128)S(1)} fusion(s32[32,12]{0,1:T(8,128)S(1)} %broadcast_in_dim.15, s32[256]{0:T(256)S(1)} %bitcast.68, s32[256]{0:T(256)S(1)} %and_select_fusion), kind=kCustom, calls=%fused_computation.5 | custom fusion | bytes 5120 | tf_op jit(solution)/shard_map/scatter | solution.py:55
  26.1 13.7 %all-to-all-start.1 = ((bf16[32,12,256]{2,1,0:T(8,128)(2,1)}), bf16[32,12,256]{2,1,0:T(8,128)(2,1)S(1)}, u32[]{:S(2)}, u32[]{:S(2)}) async-start(bf16[32,12,256]{2,1,0:T(8,128)(2,1)} %reshape.128), calls=%async_computation.1 | async-start | bytes 524288 | tf_op jit(solution)/shard_map/all_to_all | solution.py:70
  42.0 9.1 %all-to-all-done.1 = bf16[32,12,256]{2,1,0:T(8,128)(2,1)S(1)} async-done(((bf16[32,12,256]{2,1,0:T(8,128)(2,1)}), bf16[32,12,256]{2,1,0:T(8,128)(2,1)S(1)}, u32[]{:S(2)}, u32[]{:S(2)}) %all-to-all-start.1) | async-done | bytes 196640 | tf_op jit(solution)/shard_map/all_to_all | solution.py:70
  51.1 14.9 %all_to_all.40 = bf16[32,12,256]{2,1,0:T(8,128)(2,1)S(1)} all-to-all(bf16[32,12,256]{2,1,0:T(8,128)(2,1)S(1)} %reshape.136), channel_id=1, replica_groups=mesh['ep'=32,'tp'=16] {'ep'}, dimensions={0} | all-to-all | bytes 393216 | tf_op jit(solution)/shard_map/all_to_all | solution.py:71
  67.2 12.8 %scatter_fusion = f32[32,12]{0,1:T(8,128)S(1)} fusion(f32[32,12]{0,1:T(8,128)S(1)} %broadcast_in_dim.14, s32[256]{0:T(256)S(1)} %bitcast.69, f32[256]{0:T(256)S(1)} %reshape.157), kind=kCustom, calls=%fused_computation.4 | custom fusion | bytes 5120 | tf_op jit(solution)/shard_map/scatter | solution.py:60
  80.1 13.5 %all_to_all.41 = bf16[32,1,12]{2,1,0:T(2,128)(2,1)S(1)} all-to-all(bf16[32,1,12]{2,1,0:T(2,128)(2,1)S(1)} %copy.40), channel_id=1, replica_groups=mesh['ep'=32,'tp'=16] {'ep'}, dimensions={0} | all-to-all | bytes 1536 | tf_op jit(solution)/shard_map/all_to_all | solution.py:72
  93.8 41.4 %all-gather.2.cloned.1.call-done = bf16[64,12,4096]{2,1,0:T(8,128)(2,1)} async-done(((bf16[64,12,256]{2,1,0:T(8,128)(2,1)}), bf16[64,12,4096]{2,1,0:T(8,128)(2,1)}) %all-gather.2.cloned.1.call-update) | async-done | bytes 6291472 | tf_op jit(solution)/shard_map/all_gather | solution.py:13
  135.1 5.9 %fusion.17 = (bf16[32,12,4096]{2,1,0:T(8,128)(2,1)}, bf16[32,12,4096]{2,1,0:T(8,128)(2,1)}) fusion(bf16[64,12,4096]{2,1,0:T(8,128)(2,1)} %all-gather.2.cloned.1.call-done), kind=kLoop, calls=%fused_computation.55 | loop fusion | bytes 12582912 | tf_op jit(solution)/shard_map/split | solution.py:13
  141.1 5.6 %reshape.121 = bf16[384,4096]{1,0:T(8,128)(2,1)} reshape(bf16[32,12,4096]{2,1,0:T(8,128)(2,1)} %get-tuple-element.29) | data formatting | bytes 6291456 | tf_op jit(solution)/shard_map/reshape | solution.py:80
  146.7 3.1 %fusion.3 = f32[384,64]{0,1:T(8,128)S(1)} fusion(bf16[384,4096]{1,0:T(8,128)(2,1)} %reshape.121, bf16[1,64,4096]{2,1,0:T(8,128)(2,1)S(1)} %copy-done), kind=kOutput, calls=%fused_computation.17 | convolution fusion | flops 201326592 | bytes 3768320 | tf_op jit(solution)/shard_map/dot_general | solution.py:86
  150.9 5.6 %reshape.120 = bf16[384,4096]{1,0:T(8,128)(2,1)} reshape(bf16[32,12,4096]{2,1,0:T(8,128)(2,1)} %get-tuple-element.28) | data formatting | bytes 6291456 | tf_op jit(solution)/shard_map/reshape | solution.py:81
  156.6 3.0 %multiply_reduce_fusion = (f32[384]{0:T(512)S(1)}, bf16[384,64]{0,1:T(8,128)(2,1)S(1)}, bf16[384,64]{0,1:T(8,128)(2,1)S(1)}, bf16[384,64]{0,1:T(8,128)(2,1)S(1)}) fusion(f32[384,64]{0,1:T(8,128)S(1)} %fusion.6, f32[384,64]{0,1:T(8,128)S(1)} %fusion.3, f32[384]{0:T(512)S(1)} %reshape.125, bf16[384,4096]{1,0:T(8,128)(2,1)} %reshape.120, ...), kind=kOutput, calls=%fused_computation.24 | convolution fusion | flops 201793152 | bytes 4017152 | tf_op jit(solution)/shard_map/dot_general | solution.py:91
  163.3 5.5 %convert_element_type.82 = bf16[32,12,4096]{2,1,0:T(8,128)(2,1)} reshape(bf16[384,4096]{1,0:T(8,128)(2,1)} %add_convert_fusion) | data formatting | bytes 6291456 | tf_op jit(solution)/shard_map/convert_element_type | solution.py:108
  170.1 23.2 %all_to_all.42 = bf16[32,32,256]{2,1,0:T(8,128)(2,1)S(1)} all-to-all(bf16[32,32,256]{2,1,0:T(8,128)(2,1)S(1)} %bitcast.72), channel_id=1, replica_groups=mesh['ep'=32,'tp'=16] {'ep'}, dimensions={0} | all-to-all | bytes 1048576 | tf_op jit(solution)/shard_map/all_to_all | solution.py:33
  194.9 6.4 %all-to-all-start.4 = ((f32[16,1,384]{2,1,0:T(1,128)}), f32[16,1,384]{2,1,0:T(1,128)S(1)}, u32[]{:S(2)}, u32[]{:S(2)}) async-start(f32[16,1,384]{2,1,0:T(1,128)} %reshape.179), calls=%async_computation.5 | async-start | bytes 49152 | tf_op jit(solution)/shard_map/all_to_all | solution.py:18
  201.3 3.8 %convolution_bitcast_fusion = f32[1,64,4096]{2,1,0:T(8,128)} fusion(bf16[384,64]{0,1:T(8,128)(2,1)S(1)} %get-tuple-element.25, bf16[384,4096]{1,0:T(8,128)(2,1)} %reshape.120, f32[384]{0:T(512)S(1)} %reshape.125), kind=kOutput, calls=%fused_computation.8 | convolution fusion | flops 206045184 | bytes 4244992 | tf_op jit(solution)/shard_map/dot_general | solution.py:101
  205.1 3.6 %all-to-all-done.4 = f32[16,1,384]{2,1,0:T(1,128)S(1)} async-done(((f32[16,1,384]{2,1,0:T(1,128)}), f32[16,1,384]{2,1,0:T(1,128)S(1)}, u32[]{:S(2)}, u32[]{:S(2)}) %all-to-all-start.4) | async-done | bytes 24608 | tf_op jit(solution)/shard_map/all_to_all | solution.py:18
  210.7 4.3 %all-to-all-start.5 = ((bf16[32,1,12]{2,1,0:T(2,128)(2,1)}), bf16[32,1,12]{2,1,0:T(2,128)(2,1)S(1)}, u32[]{:S(2)}, u32[]{:S(2)}) async-start(bf16[32,1,12]{2,1,0:T(2,128)(2,1)} %copy.44), calls=%async_computation.6 | async-start | bytes 32768 | tf_op jit(solution)/shard_map/all_to_all | solution.py:116
  215.0 3.6 %convolution_bitcast_fusion.1 = f32[1,64,4096]{2,1,0:T(8,128)} fusion(bf16[384,64]{0,1:T(8,128)(2,1)S(1)} %get-tuple-element.31, bf16[384,4096]{1,0:T(8,128)(2,1)} %reshape.121), kind=kOutput, calls=%fused_computation.9 | convolution fusion | flops 201326592 | bytes 4243456 | tf_op jit(solution)/shard_map/dot_general | solution.py:103
  218.6 5.0 %all-to-all-done.5 = bf16[32,1,12]{2,1,0:T(2,128)(2,1)S(1)} async-done(((bf16[32,1,12]{2,1,0:T(2,128)(2,1)}), bf16[32,1,12]{2,1,0:T(2,128)(2,1)S(1)}, u32[]{:S(2)}, u32[]{:S(2)}) %all-to-all-start.5) | async-done | bytes 800 | tf_op jit(solution)/shard_map/all_to_all | solution.py:116
  223.5 5.4 %reduce-scatter.2.cloned.1.call-done = bf16[32,12,256]{2,1,0:T(8,128)(2,1)} async-done(((bf16[32,12,4096]{2,1,0:T(8,128)(2,1)}), bf16[32,12,256]{2,1,0:T(8,128)(2,1)}) %reduce-scatter.2.cloned.1.call-update) | async-done | bytes 196624 | tf_op jit(solution)/shard_map/reduce_scatter | solution.py:107
  228.9 8.8 %all-to-all-start.3 = ((bf16[32,12,256]{2,1,0:T(8,128)(2,1)}), bf16[32,12,256]{2,1,0:T(8,128)(2,1)S(1)}, u32[]{:S(2)}, u32[]{:S(2)}) async-start(bf16[32,12,256]{2,1,0:T(8,128)(2,1)} %reduce-scatter.2.cloned.1.call-done), calls=%async_computation.4 | async-start | bytes 524288 | tf_op jit(solution)/shard_map/all_to_all | solution.py:115
  237.7 3.5 %convolution_bitcast_fusion.2 = f32[1,64,4096]{2,1,0:T(8,128)} fusion(bf16[384,64]{0,1:T(8,128)(2,1)S(1)} %get-tuple-element.30, bf16[384,4096]{1,0:T(8,128)(2,1)} %reshape.121), kind=kOutput, calls=%fused_computation.10 | convolution fusion | flops 201326592 | bytes 4243456 | tf_op jit(solution)/shard_map/dot_general | solution.py:102
  244.0 4.2 %all-to-all-done.3 = bf16[32,12,256]{2,1,0:T(8,128)(2,1)S(1)} async-done(((bf16[32,12,256]{2,1,0:T(8,128)(2,1)}), bf16[32,12,256]{2,1,0:T(8,128)(2,1)S(1)}, u32[]{:S(2)}, u32[]{:S(2)}) %all-to-all-start.3) | async-done | bytes 196640 | tf_op jit(solution)/shard_map/all_to_all | solution.py:115
  (71 shorter events, 24.8 us)
Async XLA Ops:
  7.2 139.5 %copy-start = (bf16[1,64,4096]{2,1,0:T(8,128)(2,1)S(1)}, bf16[1,64,4096]{2,1,0:T(8,128)(2,1)}, u32[]{:S(2)}) copy-start(bf16[1,64,4096]{2,1,0:T(8,128)(2,1)} %param.12) | copy-start | bytes 1572868
  7.2 32.7 %copy-start.5 = (bf16[128,256]{1,0:T(8,128)(2,1)S(1)}, bf16[128,256]{1,0:T(8,128)(2,1)}, u32[]{:S(2)}) copy-start(bf16[128,256]{1,0:T(8,128)(2,1)} %param.9) | copy-start | bytes 196612
  25.3 41.6 %copy-start.6 = (f32[128,2]{0,1:T(2,128)S(1)}, f32[128,2]{0,1:T(2,128)}, u32[]{:S(2)}) copy-start(f32[128,2]{0,1:T(2,128)} %param.11) | copy-start | bytes 3076
  26.1 25.0 %all-to-all-start.1 = ((bf16[32,12,256]{2,1,0:T(8,128)(2,1)}), bf16[32,12,256]{2,1,0:T(8,128)(2,1)S(1)}, u32[]{:S(2)}, u32[]{:S(2)}) async-start(bf16[32,12,256]{2,1,0:T(8,128)(2,1)} %reshape.128), calls=%async_computation.1 | async-start | bytes 524288 | tf_op jit(solution)/shard_map/all_to_all | solution.py:70
  39.8 95.3 %all-gather.2.cloned.1.call-start = ((), (), s32[]{:S(2)}) async-start(), calls=%async_computation.8 | async-start | bytes 8912896 | tf_op jit(solution)/shard_map/all_gather | solution.py:13
  66.9 162.0 %reduce-scatter.2.cloned.1.call-start = ((), (), s32[]{:S(2)}) async-start(), calls=%async_computation.9 | async-start | bytes 4456448 | tf_op jit(solution)/shard_map/reduce_scatter | solution.py:107
  146.7 3.1 %copy-start.1 = (bf16[384,4096]{1,0:T(8,128)(2,1)S(1)}, bf16[384,4096]{1,0:T(8,128)(2,1)}, u32[]{:S(2)}) copy-start(bf16[384,4096]{1,0:T(8,128)(2,1)} %reshape.121) | copy-start | bytes 9437188
  146.7 3.1 %copy-start.2 = (bf16[1,64,4096]{2,1,0:T(8,128)(2,1)S(1)}, bf16[1,64,4096]{2,1,0:T(8,128)(2,1)}, u32[]{:S(2)}) copy-start(bf16[1,64,4096]{2,1,0:T(8,128)(2,1)} %param.13) | copy-start | bytes 1572868
  150.9 5.6 %copy-start.3 = (bf16[1,64,4096]{2,1,0:T(8,128)(2,1)S(1)}, bf16[1,64,4096]{2,1,0:T(8,128)(2,1)}, u32[]{:S(2)}) copy-start(bf16[1,64,4096]{2,1,0:T(8,128)(2,1)} %param.14) | copy-start | bytes 1572868
  168.8 0.9 copy-start.4
  194.9 13.8 %all-to-all-start.4 = ((f32[16,1,384]{2,1,0:T(1,128)}), f32[16,1,384]{2,1,0:T(1,128)S(1)}, u32[]{:S(2)}, u32[]{:S(2)}) async-start(f32[16,1,384]{2,1,0:T(1,128)} %reshape.179), calls=%async_computation.5 | async-start | bytes 49152 | tf_op jit(solution)/shard_map/all_to_all | solution.py:18
  210.7 12.8 %all-to-all-start.5 = ((bf16[32,1,12]{2,1,0:T(2,128)(2,1)}), bf16[32,1,12]{2,1,0:T(2,128)(2,1)S(1)}, u32[]{:S(2)}, u32[]{:S(2)}) async-start(bf16[32,1,12]{2,1,0:T(2,128)(2,1)} %copy.44), calls=%async_computation.6 | async-start | bytes 32768 | tf_op jit(solution)/shard_map/all_to_all | solution.py:116
  228.9 19.3 %all-to-all-start.3 = ((bf16[32,12,256]{2,1,0:T(8,128)(2,1)}), bf16[32,12,256]{2,1,0:T(8,128)(2,1)S(1)}, u32[]{:S(2)}, u32[]{:S(2)}) async-start(bf16[32,12,256]{2,1,0:T(8,128)(2,1)} %reduce-scatter.2.cloned.1.call-done), calls=%async_computation.4 | async-start | bytes 524288 | tf_op jit(solution)/shard_map/all_to_all | solution.py:115
Sparse Core Ops, SparseCore 0:
  67.0 68.0 all-gather.1
  168.9 59.9 reduce-scatter.1
where the time goes:
time: 262 us; the launch traced here: 258 us
  waiting for transfers between devices  68.6 us (26%)
  local copies, waits for them, and re-layouts  63.7 us (24%)
  blocking collectives  51.6 us (20%)
  starting transfers between devices  33.3 us (13%)
  matrix products  22.2 us (8%)
  between operations  14.4 us (5%)
  other arithmetic  4.05 us (2%)
    all_gather x1, waiting for transfers between devices, in_one_piece(): lax.all_gather(both, axis, axis=dim, tiled=True)  41.4 us
    all_to_all x1, blocking collectives, sent_and_summed(): lax.all_to_all(pieces, axis, split_axis=0, concat_axis=0, tiled=True)  23.2 us
    all_to_all x1, blocking collectives, shards(): lax.all_to_all(place_rows(cotangent), 'ep', split_axis=0, concat_axis=0,...  14.9 us
    all_to_all x1, starting transfers between devices, shards(): lax.all_to_all(place_rows(tokens), 'ep', split_axis=0, concat_axis=0, til...  13.7 us
    all_to_all x1, blocking collectives, shards(): lax.all_to_all(weight_table.astype(jnp.bfloat16), 'ep', split_axis=0, con...  13.5 us
    scatter x1, local copies, waits for them, and re-layouts, shards(): slot_table = jnp.full((experts, capacity), tok_count, jnp.int32).at[flat_...  12.8 us
    scatter x1, local copies, waits for them, and re-layouts, shards(): weight_table = jnp.zeros((experts, capacity), jnp.float32).at[flat_routes...  12.8 us
    all_to_all x1, waiting for transfers between devices, shards(): lax.all_to_all(place_rows(tokens), 'ep', split_axis=0, concat_axis=0, til...  9.12 us
  transfers between devices with their start and end apart: 6, of which 6 were waited for; matrix products, arithmetic and copies ran while one was open for 13% of the time, Pallas kernels for 0%

commit v1 on v0

v1 whole, which is shorter than its diff:
```python
import jax
import jax.numpy as jnp
import numpy as np
from jax import lax
from jax.experimental import pallas as pl
from jax.experimental.pallas import tpu as pltpu
from jax.sharding import PartitionSpec as P

MESH = pl.DeviceIdType.MESH
NZ, NX, NY = 8, 4, 8
NG = 4
ROWS = 16
BF = jnp.bfloat16
F32 = jnp.float32


def constants(blocks, cap):
    size = blocks // NG
    packed, gate_rows = size * cap, blocks // 2
    pack = np.zeros((packed, size * ROWS), np.float32)
    for q in range(size):
        for p in range(cap):
            pack[q * cap + p, q * ROWS + p] = 1
    spread = np.zeros((2, size * ROWS, size * ROWS), np.float32)
    for par in range(2):
        for q in range(size):
            for p in range(cap):
                spread[par, q * ROWS + p, gate_rows + q * cap + p] = 1
            spread[par, q * ROWS + cap, par * size + q] = 1
    total = blocks * cap
    owner = np.zeros((blocks, total), np.float32)
    place = np.zeros((total, 128), np.float32)
    for s in range(total):
        owner[s // cap, s] = 1
        place[s, s % cap] = 1
    return [jnp.asarray(a, BF) for a in (pack, spread)] + [
        jnp.asarray(owner, F32), jnp.asarray(place, BF)
    ]


def layer(cap, *refs):
    (tok, cot, routes, routes_t, gw, gw_t, shp, pack, spread, owner, place, wg, wu, wd) = refs[:14]
    (out_tok, out_gate, out_wg, out_wu, out_wd, out_sh) = refs[14:20]
    (w2, wdn, sx, sg, rx, rg, xg, shr, pre, back, gt, gn, ht, tile, ps, pr, srs, rrs) = refs[20:38]
    (fin, sb, rb, dgu, ddn, wsem, osem) = refs[38:45]
    (a2a_s, a2a_r, ag_s, ag_r, sib_s, sib_r, sh_s, sh_r) = refs[45:53]
    (pair_s, pair_r, rs_s, rs_r, rb_s, rb_r) = refs[53:]

    n_tok, feats = tok.shape
    blocks = NZ * NX
    size = blocks // NG
    vr, br, gate_rows = size * cap, size * ROWS, blocks // 2
    total = blocks * cap
    hop = NY // 2
    half = total // 2
    hid = wdn.shape[0]
    ep, tp = lax.axis_index("ep"), lax.axis_index("tp")
    z, x, y, c = ep // NX, ep % NX, tp // 2, tp % 2
    sibling = y * 2 + 1 - c

    def offset(r):
        q = r // NX
        odd = q % 2
        return (odd * ((q + 1) // 2) + (1 - odd) * (NZ - q // 2)) % NZ, r % NX

    def ahead(r):
        dz, dx = offset(r)
        return ((z + dz) % NZ) * NX + (x + dx) % NX

    def behind(r):
        dz, dx = offset(r)
        return ((z - dz + NZ) % NZ) * NX + (x - dx + NX) % NX

    def own_col(o):
        return ((y + o) % NY) * 2 + c

    def sib_col(o):
        return ((y + o) % NY) * 2 + 1 - c

    def arrived(ref, sem):
        pltpu.make_async_remote_copy(
            src_ref=ref, dst_ref=ref, send_sem=sem, recv_sem=sem,
            device_id=(ep, sibling), device_id_type=MESH,
        ).wait_recv()

    def send(src, dst, s_sem, r_sem, device):
        pltpu.make_async_remote_copy(
            src_ref=src, dst_ref=dst, send_sem=s_sem, recv_sem=r_sem,
            device_id=device, device_id_type=MESH,
        ).start()

    def dot(a, b):
        return jnp.dot(a, b, preferred_element_type=F32)

    def dot_nt(a, b):
        return lax.dot_general(a, b, (((1,), (1,)), ((), ())), preferred_element_type=F32)

    barrier = pltpu.get_barrier_semaphore()

    def greet(r, carry):
        pl.semaphore_signal(barrier, inc=1, device_id=(ahead(r), tp), device_id_type=MESH)
        return carry

    lax.fori_loop(1, blocks, greet, 0)
    for peer in (((y + 1) % NY) * 2 + c, ((y + NY - 1) % NY) * 2 + c, sibling):
        pl.semaphore_signal(barrier, inc=1, device_id=(ep, peer), device_id_type=MESH)

    loads = [
        pltpu.make_async_copy(wg.at[0], w2.at[pl.ds(0, hid)], wsem.at[0]),
        pltpu.make_async_copy(wu.at[0], w2.at[pl.ds(hid, hid)], wsem.at[1]),
        pltpu.make_async_copy(wd.at[0], wdn, wsem.at[2]),
    ]
    for load in loads:
        load.start()

    def rank_of(e):
        ez, ex = e // NX if NX & (NX - 1) else e >> (NX.bit_length() - 1), e & (NX - 1)
        dz, dx = (ez - z + NZ) & (NZ - 1), (ex - x + NX) & (NX - 1)
        q = jnp.where(dz <= NZ // 2, jnp.maximum(2 * dz - 1, 0), 2 * (NZ - dz))
        return (q * NX + dx).astype(F32)

    before = (
        lax.broadcasted_iota(jnp.int32, (n_tok, n_tok), 0)
        < lax.broadcasted_iota(jnp.int32, (n_tok, n_tok), 1)
    ).astype(F32)
    names = lax.broadcasted_iota(jnp.int32, (blocks, n_tok), 0)
    rows_e = [routes_t[k : k + 1, :] for k in range(2)]
    hot = [(names == e).astype(F32) for e in rows_e]
    seen = dot((hot[0] + hot[1]).astype(BF), before.astype(BF))
    slot_rows = [
        rank_of(rows_e[k]) * ROWS + jnp.sum(hot[k] * seen, axis=0, keepdims=True) for k in range(2)
    ]
    slots = lax.broadcasted_iota(jnp.int32, (blocks * ROWS, n_tok), 0).astype(F32)
    chosen = [(slots == d).astype(F32) for d in slot_rows]
    weight = jnp.sum(
        chosen[0] * gw_t[0:1, :] + chosen[1] * gw_t[1:2, :], axis=1, keepdims=True
    )
    table = (chosen[0] + chosen[1]).astype(BF)
    sx[...] = dot(table, tok[...]).astype(BF)
    sg[...] = (dot(table, cot[...]) * weight).astype(BF)
    rx[pl.ds(0, ROWS), :] = sx[pl.ds(0, ROWS), :]
    rg[pl.ds(0, ROWS), :] = sg[pl.ds(0, ROWS), :]

    pl.semaphore_wait(barrier, blocks - 1 + 3)

    for a, (src, dst) in enumerate(((sx, rx), (sg, rg))):
        for g in range(NG):

            def to_expert(r, carry, a=a, src=src, dst=dst, g=g):
                rows = pl.ds(pl.multiple_of(r * ROWS, ROWS), ROWS)
                send(src.at[rows], dst.at[rows], a2a_s.at[a], a2a_r.at[a, g], (ahead(r), tp))
                return carry

            lax.fori_loop(max(1, g * size), (g + 1) * size, to_expert, 0)

    def share(r, carry):
        e = ahead(r)
        n = out_sh.shape[0]
        rows = pl.ds(pl.multiple_of(e * n, n), n)
        send(shp.at[rows], shr.at[r], sh_s, sh_r, (e, tp))
        return carry

    def ring(a, way, h, k):
        d = 0 if way > 0 else 1
        part = xg.at[a, own_col(NY - h * way), pl.ds(k * half, half)]
        send(part, part, ag_s.at[a, d, h], ag_r.at[a, d, h, k], (ep, ((y + way + NY) % NY) * 2 + c))

    def to_sibling(a, o, k):
        part = xg.at[a, own_col(o), pl.ds(k * half, half)]
        send(part, part, sib_s.at[a], sib_r.at[a, o, k], (ep, sibling))

    for a, dst in enumerate((rx, rg)):
        for g in range(NG):
            lo = ROWS if g == 0 else 0
            arrived(dst.at[pl.ds(g * br + lo, br - lo)], a2a_r.at[a, g])
            got = dot(pack[...], dst[pl.ds(g * br, br), :])
            xg[a, own_col(0), pl.ds(g * vr, vr), :] = got.astype(BF)
            if g % 2 == 1:
                k = g // 2
                for way in (1, -1):
                    if hop > 1 or k == (0 if way > 0 else 1):
                        ring(a, way, 0, k)
                to_sibling(a, 0, k)
        if a == 1:
            lax.fori_loop(1, blocks, share, 0)

    for load in loads:
        load.wait()

    def forward(a, o, first=False):
        for k in range(2):
            arrived(xg.at[a, sib_col(o), pl.ds(k * half, half)], sib_r.at[a, o, k])
        acc, w = (pre, w2) if a == 0 else (back, wdn)
        part = None
        for j in (own_col(o), sib_col(o)):
            cols = pl.ds(pl.multiple_of(j * feats, feats), feats)
            term = dot_nt(w[:, cols], xg[a, j])
            part = term if part is None else part + term
        acc[...] = part if first else acc[...] + part

    for h in range(1, hop + 1):
        for a in range(2):
            for k in range(2):
                for d, way in enumerate((1, -1)):
                    if h == hop and k != d:
                        continue
                    o = (NY - h * way) % NY
                    part = xg.at[a, own_col(o), pl.ds(k * half, half)]
                    arrived(part, ag_r.at[a, d, h - 1, k])
                    if h < hop - 1 or (h == hop - 1 and k == d):
                        ring(a, way, h, k)
                    to_sibling(a, o, k)
        for a in range(2):
            if h == 1:
                forward(a, 0, first=True)
            else:
                forward(a, h - 1)
                forward(a, NY - h + 1)
    for a in range(2):
        forward(a, hop)

    s, u, b = pre[pl.ds(0, hid), :], pre[pl.ds(hid, hid), :], back[...]
    sig = 1.0 / (1.0 + jnp.exp(-s))
    silu = s * sig
    hidden = (silu * u).astype(BF)
    ht[...] = hidden
    grad_gate = b * u * sig * (1.0 + s * (1.0 - sig))
    grad_up = b * silu
    both = jnp.concatenate([grad_gate, grad_up], axis=0)
    gt[...] = both.astype(BF)
    gn[...] = both.T.astype(BF)
    gate_row = jnp.sum(hidden.astype(F32) * b, axis=0, keepdims=True)
    by_block = dot((owner[...] * gate_row).astype(BF), place[...])
    tile[...] = jnp.concatenate([by_block[:gate_rows], by_block[gate_rows:]], axis=1)

    def pair(o):
        cols = pl.ds(pl.multiple_of(sib_col(o) * feats, feats), feats)
        ps[o, pl.ds(0, gate_rows), :] = tile[...].astype(BF)
        ps[o, pl.ds(gate_rows, total), :] = dot(gn[...], w2[:, cols]).astype(BF)
        send(ps.at[o], pr.at[o], pair_s, pair_r.at[o], (ep, sibling))

    def rows_of(k):
        return pl.ds(0, gate_rows + vr) if k == 0 else pl.ds(gate_rows + k * vr, vr)

    def summed(o, k, others):
        cols = pl.ds(pl.multiple_of(own_col(o) * feats, feats), feats)
        mine = dot(gn[pl.ds(k * vr, vr), :], w2[:, cols])
        rest = pr[o, rows_of(k), :].astype(F32)
        for ref in others:
            rest = rest + ref[rows_of(k), :].astype(F32)
        if k > 0:
            return None, rest + mine
        return rest[:gate_rows] + tile[...], rest[gate_rows:] + mine

    def weights(j):
        cols = pl.ds(j * feats, feats)
        dgu[:, cols] = dot(gt[...], xg[0, j])
        ddn[:, cols] = dot(ht[...], xg[1, j])

    def rs_send(d, st, k):
        way = 1 - 2 * d
        part = pl.ds(*((0, gate_rows + vr) if k == 0 else (gate_rows + k * vr, vr)))
        send(
            srs.at[d, st, part], rrs.at[d, st, part], rs_s.at[d, st, k], rs_r.at[d, st, k],
            (ep, ((y + way + NY) % NY) * 2 + c),
        )

    started, todo = [], list(range(2 * NY))

    def some_weights(n):
        for _ in range(n):
            if todo:
                weights(todo.pop(0))

    pending = [hop] + [o for i in range(hop - 1, 0, -1) for o in (i, NY - i)] + [0]
    done = []

    def pairs_up_to(n):
        while len(done) < n:
            pair(pending[len(done)])
            done.append(1)

    ready = []

    def need(o):
        if o not in ready:
            arrived(pr.at[o], pair_r.at[o])
            ready.append(o)

    pairs_up_to(3)
    for st in range(hop):
        for k in range(NG):
            for d in range(2):
                mine = k // (NG // 2) == d
                if st == 0 and not mine:
                    continue
                way = 1 - 2 * d
                o = (way * (hop - st)) % NY
                need(o)
                others = []
                if st > 1 or (st == 1 and mine):
                    arrived(rrs.at[d, st - 1, rows_of(k)], rs_r.at[d, st - 1, k])
                    others = [rrs.at[d, st - 1]]
                gate, val = summed(o, k, others)
                if k == 0:
                    srs[d, st, pl.ds(0, gate_rows), :] = gate.astype(BF)
                srs[d, st, pl.ds(gate_rows + k * vr, vr), :] = val.astype(BF)
                rs_send(d, st, k)
                started.append((d, st, k))
            if st > 0:
                some_weights(-(-2 * NY // (NG * (hop - 1))) if hop > 1 else 2 * NY)
        pairs_up_to(NY)
        if st == 0:
            n = out_sh.shape[0]
            arrived(shp.at[pl.ds(n, (blocks - 1) * n)], sh_r)
            own = shp[pl.ds(pl.multiple_of(ep * n, n), n), :].astype(F32)
            out_sh[...] = lax.fori_loop(
                1, blocks, lambda r, acc: acc + shr[r].astype(F32), own
            )
    some_weights(2 * NY)
    stores = [
        pltpu.make_async_copy(dgu.at[pl.ds(0, hid)], out_wg.at[0], osem.at[0]),
        pltpu.make_async_copy(dgu.at[pl.ds(hid, hid)], out_wu.at[0], osem.at[1]),
        pltpu.make_async_copy(ddn, out_wd.at[0], osem.at[2]),
    ]
    for store in stores:
        store.start()

    need(0)
    gates = None
    for k in range(NG):
        for d in range(2):
            arrived(rrs.at[d, hop - 1, rows_of(k)], rs_r.at[d, hop - 1, k])
        gate, val = summed(0, k, [rrs.at[0, hop - 1], rrs.at[1, hop - 1]])
        if k == 0:
            gates = gate
        at = (k * size // gate_rows) * 128
        fin[k, pl.ds(0, gate_rows), :] = jnp.concatenate(
            [gates[:, at : at + 128], jnp.zeros((gate_rows, feats - 128), F32)], axis=1
        ).astype(BF)
        fin[k, pl.ds(gate_rows, vr), :] = val.astype(BF)
        fin[k, pl.ds(gate_rows + vr, br - gate_rows - vr), :] = jnp.zeros(
            (br - gate_rows - vr, feats), BF
        )
        sb[pl.ds(k * br, br), :] = dot(spread[k % 2], fin[k]).astype(BF)

        def home(r, carry, k=k):
            rows = pl.ds(pl.multiple_of(r * ROWS, ROWS), ROWS)
            send(sb.at[rows], rb.at[rows], rb_s, rb_r.at[k], (behind(r), tp))
            return carry

        lax.fori_loop(max(1, k * size), (k + 1) * size, home, 0)
    rb[pl.ds(0, ROWS), :] = sb[pl.ds(0, ROWS), :]

    after = (
        lax.broadcasted_iota(jnp.int32, (n_tok, n_tok), 1)
        < lax.broadcasted_iota(jnp.int32, (n_tok, n_tok), 0)
    ).astype(BF)
    names_t = lax.broadcasted_iota(jnp.int32, (n_tok, blocks), 1)
    cols_e = [routes[:, k : k + 1] for k in range(2)]
    hot_t = [(names_t == e).astype(F32) for e in cols_e]
    seen_t = dot(after, (hot_t[0] + hot_t[1]).astype(BF))
    position = [jnp.sum(hot_t[k] * seen_t, axis=1, keepdims=True) for k in range(2)]
    block = [rank_of(e) * ROWS for e in cols_e]
    slots_t = lax.broadcasted_iota(jnp.int32, (n_tok, blocks * ROWS), 1).astype(F32)
    picks = [(slots_t == block[k] + position[k]).astype(F32) for k in range(2)]
    gate_at = [(slots_t == block[k] + float(cap)).astype(BF) for k in range(2)]
    lanes = lax.broadcasted_iota(jnp.int32, (n_tok, feats), 1).astype(F32)

    for k in range(NG):
        lo = ROWS if k == 0 else 0
        arrived(rb.at[pl.ds(k * br + lo, br - lo)], rb_r.at[k])
    rows_back = rb[...]
    out_tok[...] = dot((picks[0] + picks[1]).astype(BF), rows_back).astype(BF)
    parts = []
    for k in range(2):
        found = jnp.where(lanes == position[k], dot(gate_at[k], rows_back), 0.0)
        parts.append(jnp.sum(found, axis=1, keepdims=True) / gw[:, k : k + 1])
    out_gate[...] = jnp.concatenate(parts, axis=1)

    arrived(sx.at[pl.ds(ROWS, (blocks - 1) * ROWS)], a2a_s.at[0])
    arrived(sg.at[pl.ds(ROWS, (blocks - 1) * ROWS)], a2a_s.at[1])
    arrived(shp.at[pl.ds(out_sh.shape[0], (blocks - 1) * out_sh.shape[0])], sh_s)
    for a in range(2):
        for d in range(2):
            for h in range(hop):
                n = total if h < hop - 1 else half
                arrived(xg.at[a, 0, pl.ds(0, n)], ag_s.at[a, d, h])
        arrived(xg.at[a, pl.ds(0, NY)], sib_s.at[a])
    arrived(ps, pair_s)
    for d, st, k in started:
        arrived(srs.at[d, st, rows_of(k)], rs_s.at[d, st, k])
    arrived(sb.at[pl.ds(ROWS, (blocks - 1) * ROWS)], rb_s)
    for store in stores:
        store.wait()


def shards(tokens, cotangent, routes, gate_weight, w_gate, w_up, w_down, shared_hidden):
    n_tok, feats = tokens.shape
    blocks = NZ * NX
    cap = 3 * n_tok * routes.shape[1] // (2 * blocks)
    total, size, hop = blocks * cap, blocks // NG, NY // 2
    hid, width = w_gate.shape[1:]
    chunk = total + blocks // 2
    n_sh = shared_hidden.shape[1] // blocks
    shared = jnp.dot(shared_hidden.T, cotangent, preferred_element_type=F32).astype(BF)
    dma = pltpu.SemaphoreType.DMA
    vm = pl.BlockSpec(memory_space=pltpu.VMEM)
    hbm = pl.BlockSpec(memory_space=pl.ANY)
    sent = (blocks * ROWS, feats)
    weight_out = jax.ShapeDtypeStruct((1, hid, width), F32)
    return pl.pallas_call(
        lambda *refs: layer(cap, *refs),
        out_shape=(
            jax.ShapeDtypeStruct((n_tok, feats), BF),
            jax.ShapeDtypeStruct((n_tok, 2), F32),
            weight_out,
            weight_out,
            weight_out,
            jax.ShapeDtypeStruct((n_sh, feats), F32),
        ),
        in_specs=[vm] * 11 + [hbm] * 3,
        out_specs=(vm, vm, hbm, hbm, hbm, vm),
        scratch_shapes=[
            pltpu.VMEM((2 * hid, width), BF),
            pltpu.VMEM((hid, width), BF),
            pltpu.VMEM(sent, BF),
            pltpu.VMEM(sent, BF),
            pltpu.VMEM(sent, BF),
            pltpu.VMEM(sent, BF),
            pltpu.VMEM((2, 2 * NY, total, feats), BF),
            pltpu.VMEM((blocks, n_sh, feats), BF),
            pltpu.VMEM((2 * hid, total), F32),
            pltpu.VMEM((hid, total), F32),
            pltpu.VMEM((2 * hid, total), BF),
            pltpu.VMEM((total, 2 * hid), BF),
            pltpu.VMEM((hid, total), BF),
            pltpu.VMEM((blocks // 2, feats), F32),
            pltpu.VMEM((NY, chunk, feats), BF),
            pltpu.VMEM((NY, chunk, feats), BF),
            pltpu.VMEM((2, hop, chunk, feats), BF),
            pltpu.VMEM((2, hop, chunk, feats), BF),
            pltpu.VMEM((NG, size * ROWS, feats), BF),
            pltpu.VMEM(sent, BF),
            pltpu.VMEM(sent, BF),
            pltpu.VMEM((2 * hid, width), F32),
            pltpu.VMEM((hid, width), F32),
            dma((3,)),
            dma((3,)),
            dma((2,)),
            dma((2, NG)),
            dma((2, 2, hop)),
            dma((2, 2, hop, 2)),
            dma((2,)),
            dma((2, NY, 2)),
            dma,
            dma,
            dma,
            dma((NY,)),
            dma((2, hop, NG)),
            dma((2, hop, NG)),
            dma,
            dma((NG,)),
        ],
        compiler_params=pltpu.CompilerParams(
            collective_id=0, has_side_effects=True, vmem_limit_bytes=56 * 1024 * 1024
        ),
    )(
        tokens, cotangent, routes, routes.T, gate_weight, gate_weight.T, shared,
        *constants(blocks, cap), w_gate, w_up, w_down,
    )


def solution(mesh):
    placed = (
        P("ep", "tp"),
        P("ep", "tp"),
        P("ep", None),
        P("ep", None),
        P("ep", "tp", None),
        P("ep", "tp", None),
        P("ep", "tp", None),
        P("ep", None),
    )
    return jax.shard_map(
        shards,
        mesh=mesh,
        in_specs=placed,
        out_specs=(
            P("ep", "tp"),
            P("ep", None),
            P("ep", "tp", None),
            P("ep", "tp", None),
            P("ep", "tp", None),
            P("ep", "tp"),
        ),
        check_vma=False,
    )
```

time: 262 us -> 103 us (0.39); the launches traced: 258 us -> 102 us
  Pallas kernels: 0 us -> 89.8 us
  waiting for transfers between devices: 68.6 us -> 0 us
  local copies, waits for them, and re-layouts: 63.7 us -> 9.91 us
  blocking collectives: 51.6 us -> 0 us
  starting transfers between devices: 33.3 us -> 0 us
  matrix products: 22.2 us -> 1.12 us
  between operations: 14.4 us -> 0.67 us
  other arithmetic: 4.05 us -> 0 us
    pallas_call x0 -> x1, Pallas kernels: none -> 89.8 us  [shards(): pl.pallas_call(lambda *refs: layer(cap, *refs), out_shape=(jax.ShapeDtype...]
    all_to_all x3 -> x0, blocking collectives: 51.6 us -> none  [the longest x1 23.2 us: sent_and_summed(): lax.all_to_all(pieces, axis, split_axis=0, concat_axis=0, tiled=True)]
    all_gather x1 -> x0, waiting for transfers between devices: 41.4 us -> none  [in_one_piece(): lax.all_gather(both, axis, axis=dim, tiled=True)]
    all_to_all x4 -> x0, starting transfers between devices: 33.2 us -> none  [the longest x1 13.7 us: shards(): lax.all_to_all(place_rows(tokens), 'ep', split_axis=0, concat_axis=0, til...]
    scatter x2 -> x0, local copies, waits for them, and re-layouts: 25.5 us -> none  [the longest x1 12.8 us: shards(): slot_table = jnp.full((experts, capacity), tok_count, jnp.int32).at[flat_...]
    all_to_all x4 -> x0, waiting for transfers between devices: 21.9 us -> none  [the longest x1 9.12 us: shards(): lax.all_to_all(place_rows(tokens), 'ep', split_axis=0, concat_axis=0, til...]
    dot_general x9 -> x1, matrix products: 22.2 us -> 1.12 us  [shards(): jnp.dot(shared_hidden.T, cotangent, preferred_element_type=F32).astype(BF)]
    reshape x7 -> x0, local copies, waits for them, and re-layouts: 11.8 us -> none  [the longest x1 5.63 us: shards(): rows_g = recv_cotan.reshape(row_total, width)]
  transfers between devices with their start and end apart: 6 -> 0, of which waited for: 6 -> 0; matrix products, arithmetic and copies ran while one was open for 13% -> 0% of each run, Pallas kernels for 0% -> 0%
where the time goes in v1:
time: 103 us; the launch traced here: 102 us
  Pallas kernels  89.8 us (87%)
  local copies, waits for them, and re-layouts  9.91 us (10%)
  matrix products  1.12 us (1%)
    pallas_call x1, Pallas kernels, shards(): pl.pallas_call(lambda *refs: layer(cap, *refs), out_shape=(jax.ShapeDtype...  89.8 us
    unnamed x23, local copies, waits for them, and re-layouts  8.4 us

profile of v1, /device:TPU:1, one launch (start us, length us, event | category | flops | bytes accessed | tf_op | source)
XLA Modules:
  0.0 101.5 jit_solution(13536751623783657804)
XLA Ops:
  0.6 0.0 copy-start
  0.6 0.0 copy-start.6
  0.7 0.7 copy-done.6
  1.4 0.0 copy-start.7
  1.4 0.0 copy-start.3
  1.4 0.7 copy.18.refs_2_
  2.1 0.0 copy-done.7
  2.1 0.7 copy.19.refs_4_
  2.9 0.0 copy-done
  2.9 0.0 copy-done.3
  2.9 1.1 %convolution_convert_fusion.refs_6_ = bf16[1024,256]{1,0:T(8,128)(2,1)} fusion(bf16[128,1024]{1,0:T(8,128)(2,1)S(1)} %copy-done, bf16[128,256]{1,0:T(8,128)(2,1)S(1)} %copy-done.3), kind=kOutput, calls=%fused_computation | convolution fusion | flops 67371008 | bytes 851968 | tf_op jit(solution)/shard_map/dot_general | solution.py:406
  4.0 89.8 %shard_map.163 = (bf16[128,256]{1,0:T(8,128)(2,1)}, f32[128,2]{1,0:T(8,128)}, f32[1,64,4096]{2,1,0:T(8,128)}, f32[1,64,4096]{2,1,0:T(8,128)}, f32[1,64,4096]{2,1,0:T(8,128)}, /*index=5*/f32[32,256]{1,0:T(8,128)}) custom-call(bf16[128,256]{1,0:T(8,128)(2,1)} %refs_0_.1, bf16[128,256]{1,0:T(8,128)(2,1)} %refs_1_.1, s32[128,2]{1,0:T(8,128)} %copy.18.refs_2_, ...), custom_call_target="tpu_custom_call" | custom-call | tf_op jit(solution)/shard_map/pallas_call | solution.py:412
  93.8 0.0 copy-start.4
  93.8 1.5 %copy.20 = f32[128,2]{0,1:T(2,128)} copy(f32[128,2]{1,0:T(8,128)} %get-tuple-element.7) | data formatting | bytes 2048 | tf_op jit(solution)/shard_map/pallas_call | solution.py:412
  95.3 0.0 copy-done.4
  95.4 0.6 copy.26
  96.0 0.0 copy-start.2
  96.0 2.4 %copy.27 = f32[1,64,4096]{2,1,0:T(8,128)} copy(f32[1,64,4096]{2,1,0:T(8,128)} %get-tuple-element.20) | data formatting | bytes 2097152
  98.3 0.0 copy-done.2
  98.3 1.0 copy.28
  99.3 0.6 copy-done.1
  100.0 1.0 copy.29
  100.9 0.0 copy-done.5
  100.9 0.6 copy.30
  (2 shorter events, 0.0 us)
Async XLA Ops:
  0.6 2.2 %copy-start = (bf16[128,1024]{1,0:T(8,128)(2,1)S(1)}, bf16[128,1024]{1,0:T(8,128)(2,1)}, u32[]{:S(2)}) copy-start(bf16[128,1024]{1,0:T(8,128)(2,1)} %param.19) | copy-start | bytes 786436
  0.6 0.7 copy-start.6
  1.4 0.7 copy-start.7
  1.4 1.5 %copy-start.3 = (bf16[128,256]{1,0:T(8,128)(2,1)S(1)}, bf16[128,256]{1,0:T(8,128)(2,1)}, u32[]{:S(2)}) copy-start(bf16[128,256]{1,0:T(8,128)(2,1)} %refs_1_.1) | copy-start | bytes 196612
  93.8 1.5 %copy-start.4 = (bf16[128,256]{1,0:T(8,128)(2,1)S(1)}, bf16[128,256]{1,0:T(8,128)(2,1)}, u32[]{:S(2)}) copy-start(bf16[128,256]{1,0:T(8,128)(2,1)} %get-tuple-element.18) | copy-start | bytes 196612
  96.0 2.4 %copy-start.2 = (f32[1,64,4096]{2,1,0:T(8,128)S(1)}, f32[1,64,4096]{2,1,0:T(8,128)}, u32[]{:S(2)}) copy-start(f32[1,64,4096]{2,1,0:T(8,128)} %get-tuple-element.21) | copy-start | bytes 3145732
  98.3 1.6 %copy-start.1 = (f32[1,64,4096]{2,1,0:T(8,128)S(1)}, f32[1,64,4096]{2,1,0:T(8,128)}, u32[]{:S(2)}) copy-start(f32[1,64,4096]{2,1,0:T(8,128)} %get-tuple-element.22) | copy-start | bytes 3145732
  99.9 1.0 copy-start.5

commit v2 on v1

--- a/solution.py
+++ b/solution.py
@@ -39,12 +39,13 @@
 
 
 def layer(cap, *refs):
-    (tok, cot, routes, routes_t, gw, gw_t, shp, pack, spread, owner, place, wg, wu, wd) = refs[:14]
-    (out_tok, out_gate, out_wg, out_wu, out_wd, out_sh) = refs[14:20]
-    (w2, wdn, sx, sg, rx, rg, xg, shr, pre, back, gt, gn, ht, tile, ps, pr, srs, rrs) = refs[20:38]
-    (fin, sb, rb, dgu, ddn, wsem, osem) = refs[38:45]
-    (a2a_s, a2a_r, ag_s, ag_r, sib_s, sib_r, sh_s, sh_r) = refs[45:53]
-    (pair_s, pair_r, rs_s, rs_r, rb_s, rb_r) = refs[53:]
+    (tok_in, cot_in, routes_in, gw_in, pack_in, spread_in) = refs[:6]
+    (owner_in, place_in, shid_in, wg, wu, wd) = refs[6:12]
+    (out_tok, out_gate, out_wg, out_wu, out_wd, out_sh) = refs[12:18]
+    (w2, wdn, sx, sg, rx, rg, xg, shr, pre, back, gt, gn, ht, tile, ps, pr, srs, rrs) = refs[18:36]
+    (fin, sb, rb, shp, shid, pack, spread, owner, place, tok, cot, routes_t, gw_t) = refs[36:49]
+    (wsem, a2a_s, a2a_r, ag_s, ag_r, sib_s, sib_r, sh_s, sh_r) = refs[49:58]
+    (pair_s, pair_r, rs_s, rs_r, rb_s, rb_r) = refs[58:]
 
     n_tok, feats = tok.shape
     blocks = NZ * NX
@@ -95,6 +96,15 @@
     def dot_nt(a, b):
         return lax.dot_general(a, b, (((1,), (1,)), ((), ())), preferred_element_type=F32)
 
+    firsts = [
+        pltpu.make_async_copy(src, dst, wsem.at[i])
+        for i, (src, dst) in enumerate(
+            ((routes_in, routes_t), (gw_in, gw_t), (tok_in, tok), (cot_in, cot), (pack_in, pack))
+        )
+    ]
+    for load in firsts:
+        load.start()
+
     barrier = pltpu.get_barrier_semaphore()
 
     def greet(r, carry):
@@ -106,11 +116,15 @@
         pl.semaphore_signal(barrier, inc=1, device_id=(ep, peer), device_id_type=MESH)
 
     loads = [
-        pltpu.make_async_copy(wg.at[0], w2.at[pl.ds(0, hid)], wsem.at[0]),
-        pltpu.make_async_copy(wu.at[0], w2.at[pl.ds(hid, hid)], wsem.at[1]),
-        pltpu.make_async_copy(wd.at[0], wdn, wsem.at[2]),
+        pltpu.make_async_copy(wg.at[0], w2.at[pl.ds(0, hid)], wsem.at[5]),
+        pltpu.make_async_copy(wu.at[0], w2.at[pl.ds(hid, hid)], wsem.at[6]),
+        pltpu.make_async_copy(wd.at[0], wdn, wsem.at[7]),
+        pltpu.make_async_copy(owner_in, owner, wsem.at[8]),
+        pltpu.make_async_copy(place_in, place, wsem.at[9]),
+        pltpu.make_async_copy(spread_in, spread, wsem.at[10]),
     ]
-    for load in loads:
+    load_sh = pltpu.make_async_copy(shid_in, shid, wsem.at[11])
+    for load in [load_sh, *loads]:
         load.start()
 
     def rank_of(e):
@@ -124,12 +138,14 @@
         < lax.broadcasted_iota(jnp.int32, (n_tok, n_tok), 1)
     ).astype(F32)
     names = lax.broadcasted_iota(jnp.int32, (blocks, n_tok), 0)
+    for load in firsts:
+        load.wait()
     rows_e = [routes_t[k : k + 1, :] for k in range(2)]
     hot = [(names == e).astype(F32) for e in rows_e]
     seen = dot((hot[0] + hot[1]).astype(BF), before.astype(BF))
-    slot_rows = [
-        rank_of(rows_e[k]) * ROWS + jnp.sum(hot[k] * seen, axis=0, keepdims=True) for k in range(2)
-    ]
+    block_rows = [rank_of(e) * ROWS for e in rows_e]
+    place_rows = [jnp.sum(hot[k] * seen, axis=0, keepdims=True) for k in range(2)]
+    slot_rows = [block_rows[k] + place_rows[k] for k in range(2)]
     slots = lax.broadcasted_iota(jnp.int32, (blocks * ROWS, n_tok), 0).astype(F32)
     chosen = [(slots == d).astype(F32) for d in slot_rows]
     weight = jnp.sum(
@@ -168,6 +184,12 @@
     def to_sibling(a, o, k):
         part = xg.at[a, own_col(o), pl.ds(k * half, half)]
         send(part, part, sib_s.at[a], sib_r.at[a, o, k], (ep, sibling))
+
+    load_sh.wait()
+    terms = lax.dot_general(
+        shid[...], cot[...], (((0,), (0,)), ((), ())), preferred_element_type=F32
+    )
+    shp[...] = terms.astype(BF)
 
     for a, dst in enumerate((rx, rg)):
         for g in range(NG):
@@ -254,8 +276,10 @@
 
     def weights(j):
         cols = pl.ds(j * feats, feats)
-        dgu[:, cols] = dot(gt[...], xg[0, j])
-        ddn[:, cols] = dot(ht[...], xg[1, j])
+        grads = dot(gt[...], xg[0, j])
+        out_wg[0, :, cols] = grads[:hid]
+        out_wu[0, :, cols] = grads[hid:]
+        out_wd[0, :, cols] = dot(ht[...], xg[1, j])
 
     def rs_send(d, st, k):
         way = 1 - 2 * d
@@ -318,13 +342,6 @@
                 1, blocks, lambda r, acc: acc + shr[r].astype(F32), own
             )
     some_weights(2 * NY)
-    stores = [
-        pltpu.make_async_copy(dgu.at[pl.ds(0, hid)], out_wg.at[0], osem.at[0]),
-        pltpu.make_async_copy(dgu.at[pl.ds(hid, hid)], out_wu.at[0], osem.at[1]),
-        pltpu.make_async_copy(ddn, out_wd.at[0], osem.at[2]),
-    ]
-    for store in stores:
-        store.start()
 
     need(0)
     gates = None
@@ -352,16 +369,18 @@
         lax.fori_loop(max(1, k * size), (k + 1) * size, home, 0)
     rb[pl.ds(0, ROWS), :] = sb[pl.ds(0, ROWS), :]
 
-    after = (
-        lax.broadcasted_iota(jnp.int32, (n_tok, n_tok), 1)
-        < lax.broadcasted_iota(jnp.int32, (n_tok, n_tok), 0)
-    ).astype(BF)
-    names_t = lax.broadcasted_iota(jnp.int32, (n_tok, blocks), 1)
-    cols_e = [routes[:, k : k + 1] for k in range(2)]
-    hot_t = [(names_t == e).astype(F32) for e in cols_e]
-    seen_t = dot(after, (hot_t[0] + hot_t[1]).astype(BF))
-    position = [jnp.sum(hot_t[k] * seen_t, axis=1, keepdims=True) for k in range(2)]
-    block = [rank_of(e) * ROWS for e in cols_e]
+    ones = lax.broadcasted_iota(jnp.int32, (n_tok, n_tok), 0) == lax.broadcasted_iota(
+        jnp.int32, (n_tok, n_tok), 1
+    )
+
+    def to_col(row):
+        return jnp.sum(jnp.where(ones, row, 0.0), axis=1, keepdims=True)
+
+    def to_row(col):
+        return jnp.sum(jnp.where(ones, col, 0.0), axis=0, keepdims=True)
+
+    position = [to_col(r) for r in place_rows]
+    block = [to_col(r) for r in block_rows]
     slots_t = lax.broadcasted_iota(jnp.int32, (n_tok, blocks * ROWS), 1).astype(F32)
     picks = [(slots_t == block[k] + position[k]).astype(F32) for k in range(2)]
     gate_at = [(slots_t == block[k] + float(cap)).astype(BF) for k in range(2)]
@@ -375,8 +394,8 @@
     parts = []
     for k in range(2):
         found = jnp.where(lanes == position[k], dot(gate_at[k], rows_back), 0.0)
-        parts.append(jnp.sum(found, axis=1, keepdims=True) / gw[:, k : k + 1])
-    out_gate[...] = jnp.concatenate(parts, axis=1)
+        parts.append(to_row(jnp.sum(found, axis=1, keepdims=True)))
+    out_gate[...] = jnp.concatenate(parts, axis=0) / gw_t[...]
 
     arrived(sx.at[pl.ds(ROWS, (blocks - 1) * ROWS)], a2a_s.at[0])
     arrived(sg.at[pl.ds(ROWS, (blocks - 1) * ROWS)], a2a_s.at[1])
@@ -391,8 +410,15 @@
     for d, st, k in started:
         arrived(srs.at[d, st, rows_of(k)], rs_s.at[d, st, k])
     arrived(sb.at[pl.ds(ROWS, (blocks - 1) * ROWS)], rb_s)
-    for store in stores:
-        store.wait()
+
+
+def hand_out(*refs):
+    n = len(refs) // 2
+    moves = [pltpu.make_async_copy(refs[i], refs[n + i], refs[-1].at[i]) for i in range(n)]
+    for move in moves:
+        move.start()
+    for move in moves:
+        move.wait()
 
 
 def shards(tokens, cotangent, routes, gate_weight, w_gate, w_up, w_down, shared_hidden):
@@ -403,24 +429,25 @@
     hid, width = w_gate.shape[1:]
     chunk = total + blocks // 2
     n_sh = shared_hidden.shape[1] // blocks
-    shared = jnp.dot(shared_hidden.T, cotangent, preferred_element_type=F32).astype(BF)
+    consts = constants(blocks, cap)
     dma = pltpu.SemaphoreType.DMA
     vm = pl.BlockSpec(memory_space=pltpu.VMEM)
-    hbm = pl.BlockSpec(memory_space=pl.ANY)
+    hbm = pl.BlockSpec(memory_space=pltpu.HBM)
     sent = (blocks * ROWS, feats)
     weight_out = jax.ShapeDtypeStruct((1, hid, width), F32)
-    return pl.pallas_call(
+    out_shape = (
+        jax.ShapeDtypeStruct((n_tok, feats), BF),
+        jax.ShapeDtypeStruct((2, n_tok), F32),
+        weight_out,
+        weight_out,
+        weight_out,
+        jax.ShapeDtypeStruct((n_sh, feats), F32),
+    )
+    outs = pl.pallas_call(
         lambda *refs: layer(cap, *refs),
-        out_shape=(
-            jax.ShapeDtypeStruct((n_tok, feats), BF),
-            jax.ShapeDtypeStruct((n_tok, 2), F32),
-            weight_out,
-            weight_out,
-            weight_out,
-            jax.ShapeDtypeStruct((n_sh, feats), F32),
-        ),
-        in_specs=[vm] * 11 + [hbm] * 3,
-        out_specs=(vm, vm, hbm, hbm, hbm, vm),
+        out_shape=out_shape,
+        in_specs=[hbm] * 12,
+        out_specs=(vm,) * 6,
         scratch_shapes=[
             pltpu.VMEM((2 * hid, width), BF),
             pltpu.VMEM((hid, width), BF),
@@ -443,10 +470,14 @@
             pltpu.VMEM((NG, size * ROWS, feats), BF),
             pltpu.VMEM(sent, BF),
             pltpu.VMEM(sent, BF),
-            pltpu.VMEM((2 * hid, width), F32),
-            pltpu.VMEM((hid, width), F32),
-            dma((3,)),
-            dma((3,)),
+            pltpu.VMEM((blocks * n_sh, feats), BF),
+            pltpu.VMEM(shared_hidden.shape, BF),
+            *(pltpu.VMEM(c.shape, c.dtype) for c in consts),
+            pltpu.VMEM((n_tok, feats), BF),
+            pltpu.VMEM((n_tok, feats), BF),
+            pltpu.VMEM((2, n_tok), jnp.int32),
+            pltpu.VMEM((2, n_tok), F32),
+            dma((12,)),
             dma((2,)),
             dma((2, NG)),
             dma((2, 2, hop)),
@@ -463,12 +494,25 @@
             dma((NG,)),
         ],
         compiler_params=pltpu.CompilerParams(
-            collective_id=0, has_side_effects=True, vmem_limit_bytes=56 * 1024 * 1024
+            collective_id=0, has_side_effects=True, vmem_limit_bytes=28 * 1024 * 1024
         ),
     )(
-        tokens, cotangent, routes, routes.T, gate_weight, gate_weight.T, shared,
-        *constants(blocks, cap), w_gate, w_up, w_down,
-    )
+        *(
+            pltpu.with_memory_space_constraint(a, pltpu.HBM)
+            for a in (
+                tokens, cotangent, routes.T, gate_weight.T, *consts, shared_hidden,
+                w_gate, w_up, w_down,
+            )
+        )
+    )
+    outs = pl.pallas_call(
+        hand_out,
+        out_shape=out_shape,
+        in_specs=[vm] * 6,
+        out_specs=(hbm,) * 6,
+        scratch_shapes=[dma((6,))],
+    )(*(pltpu.with_memory_space_constraint(a, pltpu.VMEM) for a in outs))
+    return (outs[0], outs[1].T, *outs[2:])
 
 
 def solution(mesh):

time: 103 us -> 92.5 us (0.90)
  local copies, waits for them, and re-layouts: 9.91 us -> 0 us
  matrix products: 1.12 us -> 0 us
    unnamed x23 -> x0, local copies, waits for them, and re-layouts: 8.4 us -> none
    pallas_call x1 -> x0, local copies, waits for them, and re-layouts: 1.51 us -> none  [shards(): pl.pallas_call(lambda *refs: layer(cap, *refs), out_shape=(jax.ShapeDtype...]
    dot_general x1 -> x0, matrix products: 1.12 us -> none  [shards(): jnp.dot(shared_hidden.T, cotangent, preferred_element_type=F32).astype(BF)]
    pallas_call x1 -> x2, Pallas kernels: 89.8 us -> 90.2 us  [the longest x1 88.5 us: shards(): pl.pallas_call(lambda *refs: layer(cap, *refs), out_shape=out_shape, in_s...]
where the time goes in v2:
time: 92.5 us; the launch traced here: 90.9 us
  Pallas kernels  90.2 us (98%)
    pallas_call x1, Pallas kernels, shards(): pl.pallas_call(lambda *refs: layer(cap, *refs), out_shape=out_shape, in_s...  88.5 us

profile of v2, /device:TPU:1, one launch (start us, length us, event | category | flops | bytes accessed | tf_op | source)
XLA Modules:
  0.0 90.9 jit_solution(17779529285946683273)
XLA Ops:
  0.6 88.5 %shard_map.163 = (bf16[128,256]{1,0:T(8,128)(2,1)S(1)}, f32[2,128]{1,0:T(2,128)S(1)}, f32[1,64,4096]{2,1,0:T(8,128)S(1)}, f32[1,64,4096]{2,1,0:T(8,128)S(1)}, f3...) custom-call(bf16[128,256]{1,0:T(8,128)(2,1)} %refs_0_.1, bf16[128,256]{1,0:T(8,128)(2,1)} %refs_1_.1, s32[2,128]{1,0:T(2,128)} %bitcast.3, ...), custom_call_target="tpu_custom_call" | custom-call | tf_op jit(solution)/shard_map/pallas_call | solution.py:446
  89.1 1.7 %shard_map.164 = (bf16[128,256]{1,0:T(8,128)(2,1)}, f32[2,128]{1,0:T(2,128)}, f32[1,64,4096]{2,1,0:T(8,128)}, f32[1,64,4096]{2,1,0:T(8,128)}, f32[1,64,4096]{2,1,0:T(8,128)}, /*index=5*/f32[32,256]{1,0:T(8,128)}) custom-call(bf16[128,256]{1,0:T(8,128)(2,1)S(1)} %get-tuple-element.18.refs_0_, f32[2,128]{1,0:T(2,128)S(1)} %get-tuple-element.19.refs_1_, ...), custom_call_target="tpu_custom_call" | custom-call | tf_op jit(solution)/shard_map/pallas_call | solution.py:508
